TPU v7x, 32 devices: a whole 2x2x4 slice. The times are simulated.
32 devices in a mesh: sp: 4 (over z), dp: 8 (over y, x, core).
Axes of the slice: x: 2, y: 2, z: 4, core: 2. Of those that a mesh axis runs over, the one named last changes fastest.
Arguments:
- query_latent: bfloat16 [8, 512, 768], P('dp', 'sp'), may hold values from -6 to 6
- keyvalue_latent: bfloat16 [8, 512, 512], P('dp', 'sp'), may hold values from -6 to 6
- rope_key: bfloat16 [8, 512, 32], P('dp', 'sp'), may hold values from -150 to 150
- query_gain: float32 [768], replicated, may hold values from 0.1 to 1.9
- keyvalue_gain: float32 [512], replicated, may hold values from 0.1 to 1.9
- narrow_query: bfloat16 [768, 384], P('dp'), may hold values from -0.21875 to 0.21875
- broad_query: bfloat16 [768, 640], P('dp'), may hold values from -0.21875 to 0.21875
- narrow_key: bfloat16 [512, 256], P('dp'), may hold values from -0.25 to 0.25
- narrow_value: bfloat16 [512, 256], P('dp'), may hold values from -0.25 to 0.25
- broad_key: bfloat16 [512, 512], P('dp'), may hold values from -0.25 to 0.25
- broad_value: bfloat16 [512, 256], P('dp'), may hold values from -0.25 to 0.25
Outputs:
- narrow_mixed: bfloat16 [8, 512, 256], P('dp', 'sp')
- broad_mixed: bfloat16 [8, 512, 256], P('dp', 'sp')
All inputs are finite; a program needn't handle non-finite values.
Results may differ from a plain program's by a relative error of at most 0.014.
The roundings to bfloat16 on the way count: a program that leaves them out, or rounds other values in their place, can miss the bound.
Values may be sent and summed in bfloat16 or wider, within the bound.
A program may use at most 64 MiB of HBM per device.

v0:
```python
import jax
import jax.numpy as jnp
from jax import lax
from jax.sharding import PartitionSpec as P

PLAIN_NARROW = 64
PLAIN_BROAD = 128
ROTARY = 32
VALUE_SIZE = 64


EPSILON = 1e-06
ROTARY_BASE = 10000.0


def normalize(latent, gain_row):
    values = latent.astype(jnp.float32)
    scaled = values * lax.rsqrt(jnp.mean(values * values, axis=-1, keepdims=True) + EPSILON)
    return (scaled * gain_row).astype(jnp.bfloat16)


def rotate(values, positions):
    halfway = ROTARY // 2
    frequency = ROTARY_BASE ** (-jnp.arange(halfway, dtype=jnp.float32) / halfway)
    angles = positions[:, None] * frequency[None, :]
    cosine = jnp.cos(angles)[:, None, :]
    sine_part = jnp.sin(angles)[:, None, :]
    width = values.shape[-1]
    plain_part = values[..., : width - ROTARY]
    first_half = values[..., width - ROTARY : width - halfway]
    second_half = values[..., width - halfway :]
    return jnp.concatenate(
        [
            plain_part,
            first_half * cosine - second_half * sine_part,
            first_half * sine_part + second_half * cosine,
        ],
        axis=-1,
    )


def make_fold(latent, pieces):
    return tuple(
        (jnp.dot(latent, weight_rows, preferred_element_type=jnp.float32) for weight_rows in pieces)
    )


def arrange(sums, width, positions, groups, with_rotary):
    row_count = positions.shape[0]
    shaped = sums.reshape(row_count, -1, width)
    if with_rotary:
        shaped = rotate(shaped, positions)
    shaped = shaped.astype(jnp.bfloat16)
    return shaped.reshape(row_count, groups, shaped.shape[1] // groups, width)


def attend_group(queries, keys_plain, values, rope_keys, factor):
    length = queries.shape[0]
    block_rows = 512
    key_whole = jnp.concatenate([keys_plain[:, 0, :], rope_keys], axis=1)
    value_head = values[:, 0, :]

    def one_block(query_block):
        scores = (
            jnp.einsum("qd,kd->qk", query_block, key_whole, preferred_element_type=jnp.float32)
            * factor
        )
        shifted = jnp.exp(scores - jnp.max(scores, axis=-1, keepdims=True))
        totals = jnp.sum(shifted, axis=-1, keepdims=True)
        mixed = jnp.dot(
            shifted.astype(jnp.bfloat16), value_head, preferred_element_type=jnp.float32
        )
        return (mixed / totals).astype(jnp.bfloat16)

    blocks = lax.map(one_block, queries[:, 0, :].reshape(length // block_rows, block_rows, -1))
    results = [blocks.reshape(length, -1)]
    return jnp.stack(results, axis=1)


def attend_both(members, rope_keys):
    query_first, key_first, value_first, query_second, key_second, value_second = members
    mixed_first = attend_group(
        query_first[:, 0],
        key_first[:, 0],
        value_first[:, 0],
        rope_keys,
        (PLAIN_NARROW + ROTARY) ** (-0.5),
    )
    mixed_second = attend_group(
        query_second[:, 0],
        key_second[:, 0],
        value_second[:, 0],
        rope_keys,
        (PLAIN_BROAD + ROTARY) ** (-0.5),
    )
    return (mixed_first[:, None], mixed_second[:, None])


def finish(mixed):
    flattened = mixed.reshape(mixed.shape[0], -1).astype(jnp.float32)
    scaled = flattened * lax.rsqrt(
        jnp.mean(flattened * flattened, axis=-1, keepdims=True) + EPSILON
    )
    return scaled.astype(jnp.bfloat16)[None]


def on_device(
    query_latent,
    keyvalue_latent,
    rope_key,
    query_gain,
    keyvalue_gain,
    narrow_query,
    broad_query,
    narrow_key,
    narrow_value,
    broad_key,
    broad_value,
):
    tokens = query_latent.shape[1]
    spread = lax.axis_size("sp")
    device_index = lax.axis_index("sp")
    width_narrow = PLAIN_NARROW + ROTARY
    width_broad = PLAIN_BROAD + ROTARY
    query_normed = normalize(query_latent[0], query_gain)
    pair_normed = normalize(keyvalue_latent[0], keyvalue_gain)
    own_positions = (device_index * tokens + jnp.arange(tokens, dtype=jnp.int32)).astype(
        jnp.float32
    )
    rope_own = rotate(rope_key[0].astype(jnp.float32)[:, None, :], own_positions)[:, 0, :].astype(
        jnp.bfloat16
    )
    query_all, pair_all, rope_all = (
        lax.all_gather(query_normed, "sp", axis=0, tiled=True),
        lax.all_gather(pair_normed, "sp", axis=0, tiled=True),
        lax.all_gather(rope_own, "sp", axis=0, tiled=True),
    )
    length = tokens * spread
    all_positions = jnp.arange(length, dtype=jnp.int32).astype(jnp.float32)

    def own_columns(weight, width):
        count = weight.shape[1] // (width * spread)
        return lax.dynamic_slice_in_dim(weight, device_index * count * width, count * width, 1)

    own_narrow_query = own_columns(narrow_query, width_narrow)
    own_broad_query = own_columns(broad_query, width_broad)
    own_narrow_key = own_columns(narrow_key, PLAIN_NARROW)
    own_narrow_value = own_columns(narrow_value, VALUE_SIZE)
    own_broad_key = own_columns(broad_key, PLAIN_BROAD)
    own_broad_value = own_columns(broad_value, VALUE_SIZE)
    query_sums = make_fold(
        query_all,
        (
            lax.all_gather(own_narrow_query, "dp", axis=0, tiled=True),
            lax.all_gather(own_broad_query, "dp", axis=0, tiled=True),
        ),
    )
    pair_sums = make_fold(
        pair_all,
        (
            lax.all_gather(own_narrow_key, "dp", axis=0, tiled=True),
            lax.all_gather(own_narrow_value, "dp", axis=0, tiled=True),
            lax.all_gather(own_broad_key, "dp", axis=0, tiled=True),
            lax.all_gather(own_broad_value, "dp", axis=0, tiled=True),
        ),
    )
    members = (
        arrange(query_sums[0], width_narrow, all_positions, 1, True),
        arrange(pair_sums[0], PLAIN_NARROW, all_positions, 1, False),
        arrange(pair_sums[1], VALUE_SIZE, all_positions, 1, False),
        arrange(query_sums[1], width_broad, all_positions, 1, True),
        arrange(pair_sums[2], PLAIN_BROAD, all_positions, 1, False),
        arrange(pair_sums[3], VALUE_SIZE, all_positions, 1, False),
    )
    mixed_first, mixed_second = attend_both(members, rope_all)
    back_first, back_second = (
        lax.all_to_all(mixed_first, "sp", split_axis=0, concat_axis=1, tiled=True),
        lax.all_to_all(mixed_second, "sp", split_axis=0, concat_axis=1, tiled=True),
    )
    return (finish(back_first), finish(back_second))


def solution(mesh):
    in_specs = (
        P("dp", "sp", None),
        P("dp", "sp", None),
        P("dp", "sp", None),
        P(),
        P(),
        P("dp", None),
        P("dp", None),
        P("dp", None),
        P("dp", None),
        P("dp", None),
        P("dp", None),
    )
    out_specs = (P("dp", "sp", None), P("dp", "sp", None))
    return jax.shard_map(
        on_device, mesh=mesh, in_specs=in_specs, out_specs=out_specs, check_vma=False
    )
```

profile of v0, /device:TPU:0, one launch (start us, length us, event | category | flops | bytes accessed | tf_op | source)
XLA Modules:
  0.0 134.5 jit_solution(1053623430203617783)
XLA Ops:
  0.7 0.8 copy-done
  1.7 10.9 %all-gather.1 = bf16[8,96,160]{1,2,0:T(8,128)(2,1)S(1)} all-gather(bf16[1,96,160]{1,2,0:T(8,128)(2,1)S(1)} %bitcast.71), channel_id=1, replica_groups=mesh['sp'=4,'dp'=8] {'dp'}, dimensions={0}, use_global_device_ids=true | all-gather | bytes 276480 | tf_op jit(solution)/shard_map/all_gather | solution.py:155
  12.7 0.1 copy.52
  12.8 0.3 reshape.397
  13.1 0.7 copy-done.1
  13.7 0.1 fusion.12
  13.9 0.6 copy-done.7
  14.5 19.8 %all_gather.27 = bf16[512,768]{1,0:T(8,128)(2,1)S(1)} all-gather(bf16[128,768]{1,0:T(8,128)(2,1)S(1)} %fusion.14), channel_id=1, replica_groups=mesh['sp'=4,'dp'=8] {'sp'}, dimensions={0}, use_global_device_ids=true | all-gather | bytes 983040 | tf_op jit(solution)/shard_map/all_gather | solution.py:134
  34.4 0.9 constant_dynamic-slice_fusion.5
  35.2 9.2 %all_gather.28 = bf16[768,96]{1,0:T(8,128)(2,1)S(1)} all-gather(bf16[96,96]{1,0:T(8,128)(2,1)S(1)} %constant_dynamic-slice_fusion.5), channel_id=1, replica_groups=mesh['sp'=4,'dp'=8] {'dp'}, dimensions={0}, use_global_device_ids=true | all-gather | bytes 165888 | tf_op jit(solution)/shard_map/all_gather | solution.py:154
  44.5 0.4 convolution_bitcast_fusion
  44.9 0.4 convolution_bitcast_fusion.1
  45.3 0.8 constant_dynamic-slice_fusion.1
  46.0 8.2 %all_gather.34 = bf16[512,128]{1,0:T(8,128)(2,1)S(1)} all-gather(bf16[64,128]{1,0:T(8,128)(2,1)S(1)} %constant_dynamic-slice_fusion.1), channel_id=1, replica_groups=mesh['sp'=4,'dp'=8] {'dp'}, dimensions={0}, use_global_device_ids=true | all-gather | bytes 147456 | tf_op jit(solution)/shard_map/all_gather | solution.py:163
  54.4 0.6 copy-done.8
  55.0 16.1 %all_gather.29 = bf16[512,512]{1,0:T(8,128)(2,1)S(1)} all-gather(bf16[128,512]{1,0:T(8,128)(2,1)S(1)} %fusion.17), channel_id=1, replica_groups=mesh['sp'=4,'dp'=8] {'sp'}, dimensions={0}, use_global_device_ids=true | all-gather | bytes 655360 | tf_op jit(solution)/shard_map/all_gather | solution.py:135
  71.1 0.7 copy-done.3
  71.8 0.1 fusion.63
  72.0 11.9 %all-gather = bf16[512,1,32]{0,2,1:T(8,128)(2,1)S(1)} all-gather(bf16[128,1,32]{0,2,1:T(8,128)(2,1)S(1)} %pad_maximum_fusion), channel_id=2, replica_groups=mesh['sp'=4,'dp'=8] {'sp'}, dimensions={0}, use_global_device_ids=true | all-gather | bytes 40960 | tf_op jit(solution)/shard_map/all_gather | solution.py:136
  83.9 9.2 %all_gather.35 = bf16[512,64]{1,0:T(8,128)(2,1)S(1)} all-gather(bf16[64,64]{1,0:T(8,128)(2,1)S(1)} %constant_dynamic-slice_fusion), channel_id=1, replica_groups=mesh['sp'=4,'dp'=8] {'dp'}, dimensions={0}, use_global_device_ids=true | all-gather | bytes 73728 | tf_op jit(solution)/shard_map/all_gather | solution.py:164
  93.1 0.2 fusion.55
  93.3 0.3 convolution_convert_fusion
  93.6 0.4 fusion.69
  94.0 0.2 fusion.6
  94.2 0.5 fusion.2
  94.6 0.5 broadcast.246
  95.2 0.7 reduce.11
  95.8 0.1 copy.59
  95.9 0.8 reshape.400
  96.7 3.3 %all-to-all-start.1 = ((bf16[4,2,4096]{2,1,0:T(2,128)(2,1)}), bf16[4,2,4096]{2,1,0:T(2,128)(2,1)S(1)}, u32[]{:S(2)}, u32[]{:S(2)}) async-start(bf16[4,2,4096]{2,1,0:T(2,128)(2,1)} %reshape.400), calls=%async_computation.1 | async-start | bytes 131072 | tf_op jit(solution)/shard_map/all_to_all | solution.py:178
  100.1 0.7 copy-done.5
  100.9 8.2 %all_gather.30 = bf16[512,64]{1,0:T(8,128)(2,1)S(1)} all-gather(bf16[64,64]{1,0:T(8,128)(2,1)S(1)} %constant_dynamic-slice_fusion.4), channel_id=1, replica_groups=mesh['sp'=4,'dp'=8] {'dp'}, dimensions={0}, use_global_device_ids=true | all-gather | bytes 73728 | tf_op jit(solution)/shard_map/all_gather | solution.py:161
  109.1 0.3 convolution_convert_fusion.3
  109.4 0.5 copy-done.6
  109.9 9.2 %all_gather.32 = bf16[512,64]{1,0:T(8,128)(2,1)S(1)} all-gather(bf16[64,64]{1,0:T(8,128)(2,1)S(1)} %constant_dynamic-slice_fusion.3), channel_id=1, replica_groups=mesh['sp'=4,'dp'=8] {'dp'}, dimensions={0}, use_global_device_ids=true | all-gather | bytes 73728 | tf_op jit(solution)/shard_map/all_gather | solution.py:162
  119.1 0.4 fusion.68
  119.5 0.2 fusion.4
  119.7 0.5 fusion.3
  120.1 0.7 reduce.10
  120.8 0.1 copy.58
  120.9 0.8 reshape.398
  121.7 5.1 %all-to-all-start = ((bf16[4,2,4096]{2,1,0:T(2,128)(2,1)}), bf16[4,2,4096]{2,1,0:T(2,128)(2,1)S(1)}, u32[]{:S(2)}, u32[]{:S(2)}) async-start(bf16[4,2,4096]{2,1,0:T(2,128)(2,1)} %reshape.398), calls=%async_computation | async-start | bytes 131072 | tf_op jit(solution)/shard_map/all_to_all | solution.py:177
  126.8 0.1 reshape.401
  126.9 0.1 copy.54
  127.1 5.4 %all-to-all-done = bf16[4,2,4096]{2,1,0:T(2,128)(2,1)S(1)} async-done(((bf16[4,2,4096]{2,1,0:T(2,128)(2,1)}), bf16[4,2,4096]{2,1,0:T(2,128)(2,1)S(1)}, u32[]{:S(2)}, u32[]{:S(2)}) %all-to-all-start) | async-done | bytes 65568 | tf_op jit(solution)/shard_map/all_to_all | solution.py:177
  132.5 0.1 reshape.399
  133.0 0.7 copy.57
  133.8 0.7 copy.56
  (42 shorter events, 1.2 us)
Async XLA Ops:
  0.6 0.9 copy-start
  12.8 0.9 copy-start.1
  13.7 0.7 copy-start.7
  45.2 9.0 %copy-start.2 = (bf16[1,128,512]{2,1,0:T(8,128)(2,1)S(1)}, bf16[1,128,512]{2,1,0:T(8,128)(2,1)}, u32[]{:S(2)}) copy-start(bf16[1,128,512]{2,1,0:T(8,128)(2,1)} %param.12) | copy-start | bytes 393220
  54.2 0.7 copy-start.8
  71.1 0.7 copy-start.3
  71.9 11.9 %copy-start.4 = (bf16[64,256]{1,0:T(8,128)(2,1)S(1)}, bf16[64,256]{1,0:T(8,128)(2,1)}, u32[]{:S(2)}) copy-start(bf16[64,256]{1,0:T(8,128)(2,1)} %param.21) | copy-start | bytes 98308
  96.7 25.0 %all-to-all-start.1 = ((bf16[4,2,4096]{2,1,0:T(2,128)(2,1)}), bf16[4,2,4096]{2,1,0:T(2,128)(2,1)S(1)}, u32[]{:S(2)}, u32[]{:S(2)}) async-start(bf16[4,2,4096]{2,1,0:T(2,128)(2,1)} %reshape.400), calls=%async_computation.1 | async-start | bytes 131072 | tf_op jit(solution)/shard_map/all_to_all | solution.py:178
  100.0 0.8 copy-start.5
  109.1 0.8 copy-start.6
  121.7 10.8 %all-to-all-start = ((bf16[4,2,4096]{2,1,0:T(2,128)(2,1)}), bf16[4,2,4096]{2,1,0:T(2,128)(2,1)S(1)}, u32[]{:S(2)}, u32[]{:S(2)}) async-start(bf16[4,2,4096]{2,1,0:T(2,128)(2,1)} %reshape.398), calls=%async_computation | async-start | bytes 131072 | tf_op jit(solution)/shard_map/all_to_all | solution.py:177
where the time goes:
time: 135 us
  blocking collectives  103 us (76%)
  local copies, waits for them, and re-layouts  11.5 us (9%)
  starting transfers between devices  8.34 us (6%)
  waiting for transfers between devices  5.39 us (4%)
  matrix products  2.99 us (2%)
  other arithmetic  2.65 us (2%)
    all_gather x1, blocking collectives, on_device(): lax.all_gather(query_normed, 'sp', axis=0, tiled=True)  19.8 us
    all_gather x1, blocking collectives, on_device(): lax.all_gather(pair_normed, 'sp', axis=0, tiled=True)  16.1 us
    all_gather x1, blocking collectives, on_device(): lax.all_gather(rope_own, 'sp', axis=0, tiled=True)  11.9 us
    all_gather x1, blocking collectives, on_device(): lax.all_gather(own_broad_query, 'dp', axis=0, tiled=True)  10.9 us
    all_gather x1, blocking collectives, on_device(): lax.all_gather(own_narrow_query, 'dp', axis=0, tiled=True)  9.23 us
    all_gather x1, blocking collectives, on_device(): lax.all_gather(own_broad_value, 'dp', axis=0, tiled=True)  9.18 us
    all_gather x1, blocking collectives, on_device(): lax.all_gather(own_narrow_value, 'dp', axis=0, tiled=True)  9.17 us
    unnamed x27, local copies, waits for them, and re-layouts  8.39 us
  transfers between devices with their start and end apart: 2, of which 1 were waited for; matrix products, arithmetic and copies ran while one was open for 3% of the time, Pallas kernels for 0%

commit v1 on v0

--- a/solution.py
+++ b/solution.py
@@ -1,6 +1,12 @@
+import functools
+import math
+
 import jax
 import jax.numpy as jnp
+import numpy as np
 from jax import lax
+from jax.experimental import pallas as pl
+from jax.experimental.pallas import tpu as pltpu
 from jax.sharding import PartitionSpec as P
 
 PLAIN_NARROW = 64
@@ -180,6 +186,422 @@
     return (finish(back_first), finish(back_second))
 
 
+MESH = pl.DeviceIdType.MESH
+ROW_TILE = 16
+LANES = 128
+NK, NV, BK, BV, NQ, BQ = range(6)
+KINDS = 9
+
+
+def rotary_tables(length):
+    halfway = ROTARY // 2
+    frequency = (
+        np.float32(ROTARY_BASE) ** (-np.arange(halfway, dtype=np.float32) / np.float32(halfway))
+    ).astype(np.float32)
+    angles = np.arange(length, dtype=np.float32)[:, None] * frequency[None, :]
+    cosine = np.cos(angles.astype(np.float64)).astype(np.float32)
+    sine = np.sin(angles.astype(np.float64)).astype(np.float32)
+    return cosine, sine
+
+
+def key_table(length):
+    cosine, sine = rotary_tables(length)
+    return np.concatenate([cosine, cosine, -sine, sine], 1)
+
+
+def wide_tables(table, plain, heads):
+    rows, halfway = table.shape[0], ROTARY // 2
+    ones = jnp.ones((rows, plain), jnp.float32)
+    zeros = jnp.zeros((rows, plain), jnp.float32)
+    zero = jnp.zeros((rows, halfway), jnp.float32)
+    keep = [ones, table[:, :ROTARY]]
+    ahead = [zeros, table[:, ROTARY : ROTARY + halfway], zero]
+    behind = [zeros, zero, table[:, ROTARY + halfway :]]
+    return [jnp.concatenate(parts * heads, axis=1) for parts in (keep, ahead, behind)]
+
+
+def fused(
+    spread,
+    heads,
+    query_hbm,
+    pair_hbm,
+    rope_hbm,
+    qgain_hbm,
+    pgain_hbm,
+    w0,
+    w1,
+    w2,
+    w3,
+    w4,
+    w5,
+    ktab_hbm,
+    narrow_out,
+    broad_out,
+    g0,
+    g1,
+    g2,
+    g3,
+    g4,
+    g5,
+    query_buf,
+    pair_buf,
+    rope_buf,
+    qgain,
+    pgain,
+    ntab,
+    btab,
+    ktab,
+    pair_normed,
+    rope_keys,
+    send_sem,
+    recv_sem,
+    zsend_sem,
+    zrecv_sem,
+    local_sem,
+    wlocal_sem,
+):
+    weights = (w0, w1, w2, w3, w4, w5)
+    gathered = (g0, g1, g2, g3, g4, g5)
+    tokens = query_hbm.shape[1]
+    z = lax.axis_index("sp")
+    me = lax.axis_index("dp")
+    core = me % 2
+    flip_p = 1 - 2 * core
+    flip_x = 2 * (1 - 2 * ((me // 2) % 2))
+    flip_y = 4 * (1 - 2 * (me // 4))
+    peer_p, peer_x, peer_y = me + flip_p, me + flip_x, me + flip_y
+    diagonal = me + flip_x + flip_y
+
+    columns_all = [w.shape[1] for w in weights]
+    pieces = [(a, 0, columns_all[a]) for a in (NK, NV, BK, BV, NQ)]
+    split = -(-(columns_all[BQ] // 2) // LANES) * LANES
+    pieces += [(BQ, 0, split), (BQ, split, columns_all[BQ] - split)]
+
+    local = [
+        pltpu.make_async_copy(pair_hbm.at[0], pair_buf.at[z], local_sem.at[0]),
+        pltpu.make_async_copy(rope_hbm.at[0], rope_buf.at[z], local_sem.at[1]),
+        pltpu.make_async_copy(query_hbm.at[0], query_buf, local_sem.at[2]),
+        pltpu.make_async_copy(qgain_hbm, qgain, local_sem.at[3]),
+        pltpu.make_async_copy(pgain_hbm, pgain, local_sem.at[4]),
+        pltpu.make_async_copy(ktab_hbm, ktab, local_sem.at[5]),
+    ]
+
+    def rows_of(array, owner, half=None):
+        rows = weights[array].shape[0]
+        if half is None:
+            return pl.ds(pl.multiple_of(owner * rows, rows), rows)
+        part = rows // 2
+        return pl.ds(pl.multiple_of(owner * rows + half * part, part), part)
+
+    own_weights = [
+        pltpu.make_async_copy(
+            weights[a], gathered[a].at[rows_of(a, me)], wlocal_sem.at[a]
+        )
+        for a in range(len(weights))
+    ]
+    for copy in local + own_weights:
+        copy.start()
+
+    barrier = pltpu.get_barrier_semaphore()
+    for peer in (peer_p, peer_x, peer_y):
+        pl.semaphore_signal(barrier, inc=1, device_id=(z, peer), device_id_type=MESH)
+
+    @pl.when(z > 0)
+    def _():
+        pl.semaphore_signal(barrier, inc=1, device_id=(z - 1, me), device_id_type=MESH)
+
+    @pl.when(z < spread - 1)
+    def _():
+        pl.semaphore_signal(barrier, inc=1, device_id=(z + 1, me), device_id_type=MESH)
+
+    line = (z + spread - 1) // spread + (2 * spread - 2 - z) // spread
+    pl.semaphore_wait(barrier, 3 + line)
+
+    chunks = 2
+    chunk_rows = tokens // chunks
+
+    def along(item, owner, step, own):
+        if item < chunks:
+            rows = pl.ds(item * chunk_rows, chunk_rows)
+            target = pair_buf.at[owner, rows]
+            source = pair_hbm.at[0, rows] if own else target
+        else:
+            target = rope_buf.at[owner]
+            source = rope_hbm.at[0] if own else target
+        return pltpu.make_async_remote_copy(
+            src_ref=source,
+            dst_ref=target,
+            send_sem=zsend_sem.at[0 if step < 0 else 1, owner, item],
+            recv_sem=zrecv_sem.at[owner, item],
+            device_id=(z + step, me),
+            device_id_type=MESH,
+        )
+
+    def send_along(owner, own, step, item):
+        @pl.when((z > 0) if step < 0 else (z < spread - 1))
+        def _():
+            along(item, owner, step, own).start()
+
+    items = range(chunks + 1)
+    for item in items:
+        for step in (-1, 1):
+            send_along(z, True, step, item)
+
+    def relay_along(distance, item):
+        for side in (1, -1):
+            owner = z + side * distance
+
+            @pl.when((owner >= 0) & (owner < spread))
+            def _():
+                along(item, owner, -side, False).wait_recv()
+                send_along(owner, False, -side, item)
+
+    def across(index, kind):
+        a, start, width = pieces[index]
+        cols = pl.ds(start, width)
+        target_of = {
+            0: (me, None, peer_p),
+            1: (me, None, peer_x),
+            2: (me, None, peer_y),
+            3: (peer_x, None, peer_p),
+            4: (peer_y, None, peer_p),
+            5: (peer_x, 0, peer_y),
+            6: (peer_y, 1, peer_x),
+            7: (diagonal, 0, peer_p),
+            8: (diagonal, 1, peer_p),
+        }
+        owner, half, device = target_of[kind]
+        target = gathered[a].at[rows_of(a, owner, half), cols]
+        source = weights[a].at[:, cols] if kind < 3 else target
+        return pltpu.make_async_remote_copy(
+            src_ref=source,
+            dst_ref=target,
+            send_sem=send_sem.at[index, kind],
+            recv_sem=recv_sem.at[index, kind],
+            device_id=(z, device),
+            device_id_type=MESH,
+        )
+
+    def arrived(index, kind):
+        a, start, width = pieces[index]
+        owner, half = {
+            0: (peer_p, None),
+            1: (peer_x, None),
+            2: (peer_y, None),
+            3: (peer_x + flip_p, None),
+            4: (peer_y + flip_p, None),
+            5: (diagonal, 0),
+            6: (diagonal, 1),
+            7: (diagonal + flip_p, 0),
+            8: (diagonal + flip_p, 1),
+        }[kind]
+        target = gathered[a].at[rows_of(a, owner, half), pl.ds(start, width)]
+        pltpu.make_async_remote_copy(
+            src_ref=target,
+            dst_ref=target,
+            send_sem=send_sem.at[index, kind],
+            recv_sem=recv_sem.at[index, kind],
+            device_id=(z, peer_p),
+            device_id_type=MESH,
+        ).wait_recv()
+
+    def send_own(index):
+        for kind in (1, 2, 0):
+            across(index, kind).start()
+
+    def relay(index):
+        arrived(index, 1)
+        across(index, 5).start()
+        across(index, 3).start()
+        arrived(index, 2)
+        across(index, 6).start()
+        across(index, 4).start()
+
+    def hand_over(index):
+        for half in (0, 1):
+            arrived(index, 5 + half)
+            across(index, 7 + half).start()
+
+    def complete(index):
+        for kind in (0, 3, 4, 7, 8):
+            arrived(index, kind)
+
+    for index in range(4):
+        send_own(index)
+
+    def normed(values, gain):
+        values = values.astype(jnp.float32)
+        scaled = values * lax.rsqrt(jnp.mean(values * values, axis=-1, keepdims=True) + EPSILON)
+        return (scaled * gain).astype(jnp.bfloat16)
+
+    for copy in local:
+        copy.wait()
+    for copy in own_weights:
+        copy.wait()
+    query_normed = normed(query_buf[...], qgain[...])
+    own_table = ktab[pl.ds(pl.multiple_of(z * tokens, tokens), tokens)]
+    for table, plain in ((ntab, PLAIN_NARROW), (btab, PLAIN_BROAD)):
+        for index, values in enumerate(wide_tables(own_table, plain, heads)):
+            table[index] = values
+
+    relay(0)
+    send_own(4)
+    for item in items:
+        relay_along(1, item)
+    relay(1)
+    relay(2)
+    relay(3)
+    hand_over(0)
+    send_own(5)
+    send_own(6)
+    hand_over(1)
+    hand_over(2)
+    for distance in range(2, spread):
+        for item in items:
+            relay_along(distance, item)
+    hand_over(3)
+    relay(4)
+    relay(5)
+    relay(6)
+    for index in range(4):
+        complete(index)
+
+    for block in range(spread):
+        rows = pl.ds(block * tokens, tokens)
+        pair_normed[rows] = normed(pair_buf[block], pgain[...])
+        plain = rope_buf[block].astype(jnp.float32)
+        halfway = ROTARY // 2
+        swapped = jnp.concatenate([plain[:, halfway:], plain[:, :halfway]], axis=1)
+        rope_keys[rows] = (
+            plain * ktab[rows, :ROTARY] + swapped * ktab[rows, ROTARY:]
+        ).astype(jnp.bfloat16)
+
+    def product(left, right):
+        return jnp.dot(left, right, preferred_element_type=jnp.float32)
+
+    narrow_keys = product(pair_normed[...], g0[...]).astype(jnp.bfloat16)
+    narrow_values = product(pair_normed[...], g1[...]).astype(jnp.bfloat16)
+    hand_over(4)
+    broad_keys = product(pair_normed[...], g2[...]).astype(jnp.bfloat16)
+    broad_values = product(pair_normed[...], g3[...]).astype(jnp.bfloat16)
+    hand_over(5)
+    hand_over(6)
+
+    def attend(query_weights, table, keys, values, plain, out):
+        width = plain + ROTARY
+        sums = product(query_normed, query_weights[...])
+        total = sums.shape[1]
+        halfway = ROTARY // 2
+        queries = (
+            sums * table[0]
+            + pltpu.roll(sums, total - halfway, 1) * table[1]
+            + pltpu.roll(sums, halfway, 1) * table[2]
+        ).astype(jnp.bfloat16)
+        factor = width ** (-0.5) * math.log2(math.e)
+        attended = []
+        for head in range(heads):
+            query = queries[:, head * width : (head + 1) * width]
+            key = jnp.concatenate(
+                [keys[:, head * plain : (head + 1) * plain], rope_keys[...]], axis=1
+            )
+            scores = lax.dot_general(
+                query, key, (((1,), (1,)), ((), ())), preferred_element_type=jnp.float32
+            )
+            shifted = jnp.exp2((scores - jnp.max(scores, axis=-1, keepdims=True)) * factor)
+            totals = jnp.sum(shifted, axis=-1, keepdims=True)
+            mixed = product(
+                shifted.astype(jnp.bfloat16), values[:, head * VALUE_SIZE : (head + 1) * VALUE_SIZE]
+            )
+            attended.append((mixed / totals).astype(jnp.bfloat16).astype(jnp.float32))
+        flat = jnp.concatenate(attended, axis=1)
+        scaled = flat * lax.rsqrt(jnp.mean(flat * flat, axis=-1, keepdims=True) + EPSILON)
+        out[0] = scaled.astype(jnp.bfloat16)
+
+    complete(4)
+    attend(g4, ntab, narrow_keys, narrow_values, PLAIN_NARROW, narrow_out)
+    complete(5)
+    complete(6)
+    attend(g5, btab, broad_keys, broad_values, PLAIN_BROAD, broad_out)
+
+    for index in range(len(pieces)):
+        for kind in range(KINDS):
+            across(index, kind).wait_send()
+    for item in items:
+        for step in (-1, 1):
+            for distance in range(spread):
+                owner = z - step * distance
+
+                @pl.when(
+                    (owner >= 0)
+                    & (owner < spread)
+                    & ((z > 0) if step < 0 else (z < spread - 1))
+                )
+                def _():
+                    along(item, owner, step, False).wait_send()
+
+
+def fused_call(
+    spread,
+    query_latent,
+    keyvalue_latent,
+    rope_key,
+    query_gain,
+    keyvalue_gain,
+    narrow_query,
+    broad_query,
+    narrow_key,
+    narrow_value,
+    broad_key,
+    broad_value,
+):
+    tokens, query_rank = query_latent.shape[1:]
+    pair_rank = keyvalue_latent.shape[2]
+    length = tokens * spread
+    heads = narrow_value.shape[1] // VALUE_SIZE
+    weights = (narrow_key, narrow_value, broad_key, broad_value, narrow_query, broad_query)
+    peers = lax.axis_size("dp")
+    ktab = key_table(length)
+    operands = (
+        query_latent,
+        keyvalue_latent,
+        rope_key,
+        query_gain[None],
+        keyvalue_gain[None],
+        *weights,
+        jnp.asarray(ktab),
+    )
+    out = jax.ShapeDtypeStruct((1, tokens, heads * VALUE_SIZE), jnp.bfloat16)
+    bf16, f32 = jnp.bfloat16, jnp.float32
+    return pl.pallas_call(
+        functools.partial(fused, spread, heads),
+        out_shape=(out, out),
+        in_specs=[pl.BlockSpec(memory_space=pl.ANY)] * len(operands),
+        out_specs=[pl.BlockSpec(memory_space=pltpu.VMEM)] * 2,
+        scratch_shapes=[
+            *[pltpu.VMEM((w.shape[0] * peers, w.shape[1]), bf16) for w in weights],
+            pltpu.VMEM((tokens, query_rank), bf16),
+            pltpu.VMEM((spread, tokens, pair_rank), bf16),
+            pltpu.VMEM((spread, tokens, ROTARY), bf16),
+            pltpu.VMEM((1, query_rank), f32),
+            pltpu.VMEM((1, pair_rank), f32),
+            pltpu.VMEM((3, tokens, narrow_query.shape[1]), f32),
+            pltpu.VMEM((3, tokens, broad_query.shape[1]), f32),
+            pltpu.VMEM(ktab.shape, f32),
+            pltpu.VMEM((length, pair_rank), bf16),
+            pltpu.VMEM((length, ROTARY), bf16),
+            pltpu.SemaphoreType.DMA((7, KINDS)),
+            pltpu.SemaphoreType.DMA((7, KINDS)),
+            pltpu.SemaphoreType.DMA((2, spread, 3)),
+            pltpu.SemaphoreType.DMA((spread, 3)),
+            pltpu.SemaphoreType.DMA((6,)),
+            pltpu.SemaphoreType.DMA((6,)),
+        ],
+        compiler_params=pltpu.CompilerParams(
+            collective_id=0, has_side_effects=True, vmem_limit_bytes=48 * 2**20
+        ),
+    )(*operands)
+
+
 def solution(mesh):
     in_specs = (
         P("dp", "sp", None),
@@ -195,6 +617,15 @@
         P("dp", None),
     )
     out_specs = (P("dp", "sp", None), P("dp", "sp", None))
+    spread = mesh.shape["sp"]
+
+    def choose(*arrays):
+        rows = [a.shape[0] for a in arrays[5:]]
+        fits = lax.axis_size("dp") == 2**3 and all(r % (2 * ROW_TILE) == 0 for r in rows)
+        if fits:
+            return fused_call(spread, *arrays)
+        return on_device(*arrays)
+
     return jax.shard_map(
-        on_device, mesh=mesh, in_specs=in_specs, out_specs=out_specs, check_vma=False
-    )
+        choose, mesh=mesh, in_specs=in_specs, out_specs=out_specs, check_vma=False
+    )

time: 135 us -> 39.4 us (0.29)
  blocking collectives: 103 us -> 0 us
  Pallas kernels: 0 us -> 28.5 us
  starting transfers between devices: 8.34 us -> 0 us
  waiting for transfers between devices: 5.39 us -> 0 us
  matrix products: 2.99 us -> 0 us
  other arithmetic: 2.65 us -> 0 us
  local copies, waits for them, and re-layouts: 11.5 us -> 9.7 us
    all_gather x9 -> x0, blocking collectives: 103 us -> none  [the longest x1 19.8 us: on_device(): lax.all_gather(query_normed, 'sp', axis=0, tiled=True)]
    pallas_call x0 -> x1, Pallas kernels: none -> 28.5 us  [fused_call(): pl.pallas_call(functools.partial(fused, spread, heads), out_shape=(out, o...]
    all_to_all x2 -> x0, starting transfers between devices: 8.34 us -> none  [the longest x1 5.06 us: on_device(): lax.all_to_all(mixed_first, 'sp', split_axis=0, concat_axis=1, tiled=True)]
    all_to_all x2 -> x0, waiting for transfers between devices: 5.39 us -> none  [the longest x1 5.38 us: on_device(): lax.all_to_all(mixed_first, 'sp', split_axis=0, concat_axis=1, tiled=True)]
    dot_general x8 -> x0, matrix products: 2.99 us -> none  [the longest x4 1.37 us: make_fold(): jnp.dot(latent, weight_rows, preferred_element_type=jnp.float32)]
    dynamic_slice x7 -> x0, local copies, waits for them, and re-layouts: 2.06 us -> none  [own_columns(): lax.dynamic_slice_in_dim(weight, device_index * count * width, count * wi...]
    another operation x3 -> x0, other arithmetic: 1.44 us -> none  [the longest x2 1.32 us: attend_both(): return (mixed_first[:, None], mixed_second[:, None])]
    unnamed x27 -> x23, local copies, waits for them, and re-layouts: 8.39 us -> 9.01 us
  transfers between devices with their start and end apart: 2 -> 0, of which waited for: 1 -> 0; matrix products, arithmetic and copies ran while one was open for 3% -> 0% of each run, Pallas kernels for 0% -> 0%
where the time goes in v1:
time: 39.4 us; the launch traced here: 38.8 us
  Pallas kernels  28.5 us (72%)
  local copies, waits for them, and re-layouts  9.7 us (25%)
  between operations  0.67 us (2%)
    pallas_call x1, Pallas kernels, fused_call(): pl.pallas_call(functools.partial(fused, spread, heads), out_shape=(out, o...  28.5 us
    unnamed x23, local copies, waits for them, and re-layouts  9.01 us

profile of v1, /device:TPU:0, one launch (start us, length us, event | category | flops | bytes accessed | tf_op | source)
XLA Modules:
  0.0 38.8 jit_solution(16444709209292880840)
XLA Ops:
  0.6 0.0 copy-start.6
  0.6 0.7 %broadcast_in_dim.6.qgain_hbm = f32[1,768]{1,0:T(1,128)S(1)} reshape(f32[768]{0:T(1024)} %param.15) | data formatting | bytes 6144 | tf_op jit(solution)/shard_map/broadcast_in_dim | solution.py:568
  1.3 0.0 copy-start.9
  1.3 0.8 %copy.14.rope_hbm = bf16[1,128,32]{2,1,0:T(8,128)(2,1)S(1)} copy(bf16[1,128,32]{1,2,0:T(8,128)(2,1)} %param.14) | data formatting | bytes 16384 | tf_op args[2]
  2.2 0.0 copy-done.6
  2.2 0.0 copy-done.9
  2.2 0.0 copy-start
  2.2 0.9 %copy-done = f32[512,64]{1,0:T(8,128)S(1)} copy-done((f32[512,64]{1,0:T(8,128)S(1)}, f32[512,64]{1,0:T(8,128)}, u32[]{:S(2)}) %copy-start) | copy-done | bytes 131096
  3.1 0.0 copy-start.1
  3.1 0.9 %copy-done.1 = bf16[1,128,768]{2,1,0:T(8,128)(2,1)S(1)} copy-done((bf16[1,128,768]{2,1,0:T(8,128)(2,1)S(1)}, bf16[1,128,768]{2,1,0:T(8,128)(2,1)}, u32[]{:S(2)}) %copy-start.1) | copy-done | bytes 196632
  4.1 0.0 copy-start.2
  4.1 0.9 %copy-done.2 = bf16[1,128,512]{2,1,0:T(8,128)(2,1)S(1)} copy-done((bf16[1,128,512]{2,1,0:T(8,128)(2,1)S(1)}, bf16[1,128,512]{2,1,0:T(8,128)(2,1)}, u32[]{:S(2)}) %copy-start.2) | copy-done | bytes 131096
  5.0 0.0 copy-start.3
  5.0 0.9 %copy-done.3 = bf16[96,640]{1,0:T(8,128)(2,1)S(1)} copy-done((bf16[96,640]{1,0:T(8,128)(2,1)S(1)}, bf16[96,640]{1,0:T(8,128)(2,1)}, u32[]{:S(2)}) %copy-start.3) | copy-done | bytes 122904
  5.9 0.0 copy-start.4
  5.9 0.9 %copy-done.4 = bf16[96,384]{1,0:T(8,128)(2,1)S(1)} copy-done((bf16[96,384]{1,0:T(8,128)(2,1)S(1)}, bf16[96,384]{1,0:T(8,128)(2,1)}, u32[]{:S(2)}) %copy-start.4) | copy-done | bytes 73752
  6.7 0.0 copy-start.5
  6.8 0.8 %copy-done.5 = bf16[64,512]{1,0:T(8,128)(2,1)S(1)} copy-done((bf16[64,512]{1,0:T(8,128)(2,1)S(1)}, bf16[64,512]{1,0:T(8,128)(2,1)}, u32[]{:S(2)}) %copy-start.5) | copy-done | bytes 65560
  7.6 0.0 copy-start.7
  7.6 0.8 %copy-done.7 = bf16[64,256]{1,0:T(8,128)(2,1)S(1)} copy-done((bf16[64,256]{1,0:T(8,128)(2,1)S(1)}, bf16[64,256]{1,0:T(8,128)(2,1)}, u32[]{:S(2)}) %copy-start.7) | copy-done | bytes 32792
  8.3 0.0 copy-start.8
  8.3 0.8 %copy-done.8 = bf16[64,256]{1,0:T(8,128)(2,1)S(1)} copy-done((bf16[64,256]{1,0:T(8,128)(2,1)S(1)}, bf16[64,256]{1,0:T(8,128)(2,1)}, u32[]{:S(2)}) %copy-start.8) | copy-done | bytes 32792
  9.1 28.5 %shard_map.131 = (bf16[1,128,256]{2,1,0:T(8,128)(2,1)S(1)}, bf16[1,128,256]{2,1,0:T(8,128)(2,1)S(1)}) custom-call(bf16[1,128,768]{2,1,0:T(8,128)(2,1)S(1)} %copy-done.1, bf16[1,128,512]{2,1,0:T(8,128)(2,1)S(1)} %copy-done.2, bf16[1,128,32]{2,1,0:T(8,128)(2,1)S(1)} %copy.14.rope_hbm, f32[1,768]{1,0:T(1,128)S(1)} %broadcast_in_dim.6.qgain_hbm, ...), custom_call_target="tpu_custom_call" | custom-call | tf_op jit(solution)/shard_map/pallas_call | solution.py:575
  37.6 0.6 %copy.17 = bf16[1,128,256]{2,1,0:T(8,128)(2,1)} copy(bf16[1,128,256]{2,1,0:T(8,128)(2,1)S(1)} %get-tuple-element.4) | data formatting | bytes 131072
  38.2 0.6 %copy.18 = bf16[1,128,256]{2,1,0:T(8,128)(2,1)} copy(bf16[1,128,256]{2,1,0:T(8,128)(2,1)S(1)} %get-tuple-element.5) | data formatting | bytes 131072
Async XLA Ops:
  0.6 1.5 %copy-start.6 = (bf16[64,256]{1,0:T(8,128)(2,1)S(1)}, bf16[64,256]{1,0:T(8,128)(2,1)}, u32[]{:S(2)}) copy-start(bf16[64,256]{1,0:T(8,128)(2,1)} %w0.1) | copy-start | bytes 98308
  1.3 0.8 %copy-start.9 = (f32[512]{0:T(512)S(1)}, f32[512]{0:T(512)}, u32[]{:S(2)}) copy-start(f32[512]{0:T(512)} %param.16) | copy-start | bytes 6148
  2.2 1.0 %copy-start = (f32[512,64]{1,0:T(8,128)S(1)}, f32[512,64]{1,0:T(8,128)}, u32[]{:S(2)}) copy-start(f32[512,64]{1,0:T(8,128)} %constant.2.clone.ktab_hbm) | copy-start | bytes 393220
  3.1 0.9 %copy-start.1 = (bf16[1,128,768]{2,1,0:T(8,128)(2,1)S(1)}, bf16[1,128,768]{2,1,0:T(8,128)(2,1)}, u32[]{:S(2)}) copy-start(bf16[1,128,768]{2,1,0:T(8,128)(2,1)} %query_hbm.1) | copy-start | bytes 589828
  4.1 0.9 %copy-start.2 = (bf16[1,128,512]{2,1,0:T(8,128)(2,1)S(1)}, bf16[1,128,512]{2,1,0:T(8,128)(2,1)}, u32[]{:S(2)}) copy-start(bf16[1,128,512]{2,1,0:T(8,128)(2,1)} %pair_hbm.1) | copy-start | bytes 393220
  5.0 0.9 %copy-start.3 = (bf16[96,640]{1,0:T(8,128)(2,1)S(1)}, bf16[96,640]{1,0:T(8,128)(2,1)}, u32[]{:S(2)}) copy-start(bf16[96,640]{1,0:T(8,128)(2,1)} %w5.1) | copy-start | bytes 368644
  5.9 0.9 %copy-start.4 = (bf16[96,384]{1,0:T(8,128)(2,1)S(1)}, bf16[96,384]{1,0:T(8,128)(2,1)}, u32[]{:S(2)}) copy-start(bf16[96,384]{1,0:T(8,128)(2,1)} %w4.1) | copy-start | bytes 221188
  6.7 0.8 %copy-start.5 = (bf16[64,512]{1,0:T(8,128)(2,1)S(1)}, bf16[64,512]{1,0:T(8,128)(2,1)}, u32[]{:S(2)}) copy-start(bf16[64,512]{1,0:T(8,128)(2,1)} %w2.1) | copy-start | bytes 196612
  7.6 0.8 %copy-start.7 = (bf16[64,256]{1,0:T(8,128)(2,1)S(1)}, bf16[64,256]{1,0:T(8,128)(2,1)}, u32[]{:S(2)}) copy-start(bf16[64,256]{1,0:T(8,128)(2,1)} %w1.1) | copy-start | bytes 98308
  8.3 0.8 %copy-start.8 = (bf16[64,256]{1,0:T(8,128)(2,1)S(1)}, bf16[64,256]{1,0:T(8,128)(2,1)}, u32[]{:S(2)}) copy-start(bf16[64,256]{1,0:T(8,128)(2,1)} %w3.1) | copy-start | bytes 98308

commit v2 on v1

--- a/solution.py
+++ b/solution.py
@@ -281,8 +281,8 @@
         pltpu.make_async_copy(pair_hbm.at[0], pair_buf.at[z], local_sem.at[0]),
         pltpu.make_async_copy(rope_hbm.at[0], rope_buf.at[z], local_sem.at[1]),
         pltpu.make_async_copy(query_hbm.at[0], query_buf, local_sem.at[2]),
-        pltpu.make_async_copy(qgain_hbm, qgain, local_sem.at[3]),
-        pltpu.make_async_copy(pgain_hbm, pgain, local_sem.at[4]),
+        pltpu.make_async_copy(qgain_hbm, qgain.at[0], local_sem.at[3]),
+        pltpu.make_async_copy(pgain_hbm, pgain.at[0], local_sem.at[4]),
         pltpu.make_async_copy(ktab_hbm, ktab, local_sem.at[5]),
     ]
 
@@ -469,7 +469,7 @@
     for block in range(spread):
         rows = pl.ds(block * tokens, tokens)
         pair_normed[rows] = normed(pair_buf[block], pgain[...])
-        plain = rope_buf[block].astype(jnp.float32)
+        plain = rope_buf[block].astype(jnp.float32).T
         halfway = ROTARY // 2
         swapped = jnp.concatenate([plain[:, halfway:], plain[:, :halfway]], axis=1)
         rope_keys[rows] = (
@@ -564,9 +564,9 @@
     operands = (
         query_latent,
         keyvalue_latent,
-        rope_key,
-        query_gain[None],
-        keyvalue_gain[None],
+        jnp.swapaxes(rope_key, 1, 2),
+        query_gain,
+        keyvalue_gain,
         *weights,
         jnp.asarray(ktab),
     )
@@ -575,13 +575,13 @@
     return pl.pallas_call(
         functools.partial(fused, spread, heads),
         out_shape=(out, out),
-        in_specs=[pl.BlockSpec(memory_space=pl.ANY)] * len(operands),
+        in_specs=[pl.BlockSpec(memory_space=pltpu.HBM)] * len(operands),
         out_specs=[pl.BlockSpec(memory_space=pltpu.VMEM)] * 2,
         scratch_shapes=[
             *[pltpu.VMEM((w.shape[0] * peers, w.shape[1]), bf16) for w in weights],
             pltpu.VMEM((tokens, query_rank), bf16),
             pltpu.VMEM((spread, tokens, pair_rank), bf16),
-            pltpu.VMEM((spread, tokens, ROTARY), bf16),
+            pltpu.VMEM((spread, ROTARY, tokens), bf16),
             pltpu.VMEM((1, query_rank), f32),
             pltpu.VMEM((1, pair_rank), f32),
             pltpu.VMEM((3, tokens, narrow_query.shape[1]), f32),
@@ -597,7 +597,7 @@
             pltpu.SemaphoreType.DMA((6,)),
         ],
         compiler_params=pltpu.CompilerParams(
-            collective_id=0, has_side_effects=True, vmem_limit_bytes=48 * 2**20
+            collective_id=0, has_side_effects=True, vmem_limit_bytes=60 * 2**20
         ),
     )(*operands)
 

time: 39.4 us -> 30.7 us (0.78)
  local copies, waits for them, and re-layouts: 9.7 us -> 2.14 us
  Pallas kernels: 28.5 us -> 27.7 us
    unnamed x23 -> x4, local copies, waits for them, and re-layouts: 9.01 us -> 2.14 us
    pallas_call x1, Pallas kernels: 28.5 us -> 27.7 us  [fused_call(): pl.pallas_call(functools.partial(fused, spread, heads), out_shape=(out, o...]
    broadcast_in_dim x1 -> x0, local copies, waits for them, and re-layouts: 0.7 us -> none  [fused_call(): query_gain[None]]
where the time goes in v2:
time: 30.7 us; the launch traced here: 30.5 us
  Pallas kernels  27.7 us (90%)
  local copies, waits for them, and re-layouts  2.14 us (7%)
  between operations  0.65 us (2%)
    pallas_call x1, Pallas kernels, fused_call(): pl.pallas_call(functools.partial(fused, spread, heads), out_shape=(out, o...  27.7 us
    unnamed x4, local copies, waits for them, and re-layouts  2.14 us

profile of v2, /device:TPU:0, one launch (start us, length us, event | category | flops | bytes accessed | tf_op | source)
XLA Modules:
  0.0 30.5 jit_solution(10068216580367008829)
XLA Ops:
  0.6 27.7 %shard_map.131 = (bf16[1,128,256]{2,1,0:T(8,128)(2,1)}, bf16[1,128,256]{2,1,0:T(8,128)(2,1)}) custom-call(bf16[1,128,768]{2,1,0:T(8,128)(2,1)} %query_hbm.1, bf16[1,128,512]{2,1,0:T(8,128)(2,1)} %pair_hbm.1, bf16[1,32,128]{2,1,0:T(8,128)(2,1)} %bitcast.1, f32[768]{0:T(1024)} %qgain_hbm.1, f32[512]{0:T(512)} %pgain_hbm.1, bf16[64,256]{1,0:T(8,128)(2,1)} %w0.1, ...), custom_call_target="tpu_custom_call" | custom-call | tf_op jit(solution)/shard_map/pallas_call | solution.py:575
  28.4 0.0 copy-start
  28.4 1.5 %copy.16 = bf16[1,128,256]{2,1,0:T(8,128)(2,1)} copy(bf16[1,128,256]{2,1,0:T(8,128)(2,1)} %get-tuple-element.4) | data formatting | bytes 131072
  29.9 0.0 copy-done
  29.9 0.6 %copy.17 = bf16[1,128,256]{2,1,0:T(8,128)(2,1)} copy(bf16[1,128,256]{2,1,0:T(8,128)(2,1)S(1)} %copy-done) | data formatting | bytes 131072
Async XLA Ops:
  28.4 1.5 %copy-start = (bf16[1,128,256]{2,1,0:T(8,128)(2,1)S(1)}, bf16[1,128,256]{2,1,0:T(8,128)(2,1)}, u32[]{:S(2)}) copy-start(bf16[1,128,256]{2,1,0:T(8,128)(2,1)} %get-tuple-element.5) | copy-start | bytes 196612

commit v3 on v2

--- a/solution.py
+++ b/solution.py
@@ -189,7 +189,7 @@
 MESH = pl.DeviceIdType.MESH
 ROW_TILE = 16
 LANES = 128
-NK, NV, BK, BV, NQ, BQ = range(6)
+NK, NV, NQ, BK, BV, BQ = range(6)
 KINDS = 9
 
 
@@ -253,6 +253,8 @@
     ktab,
     pair_normed,
     rope_keys,
+    narrow_sums,
+    broad_sums,
     send_sem,
     recv_sem,
     zsend_sem,
@@ -273,7 +275,7 @@
     diagonal = me + flip_x + flip_y
 
     columns_all = [w.shape[1] for w in weights]
-    pieces = [(a, 0, columns_all[a]) for a in (NK, NV, BK, BV, NQ)]
+    pieces = [(a, 0, columns_all[a]) for a in (NK, NV, NQ, BK, BV)]
     split = -(-(columns_all[BQ] // 2) // LANES) * LANES
     pieces += [(BQ, 0, split), (BQ, split, columns_all[BQ] - split)]
 
@@ -446,24 +448,25 @@
 
     relay(0)
     send_own(4)
+    relay(1)
     for item in items:
         relay_along(1, item)
-    relay(1)
     relay(2)
     relay(3)
-    hand_over(0)
     send_own(5)
     send_own(6)
+    hand_over(0)
     hand_over(1)
+    for item in items:
+        relay_along(2, item)
+    relay(4)
     hand_over(2)
-    for distance in range(2, spread):
+    for distance in range(3, spread):
         for item in items:
             relay_along(distance, item)
     hand_over(3)
-    relay(4)
     relay(5)
-    relay(6)
-    for index in range(4):
+    for index in range(3):
         complete(index)
 
     for block in range(spread):
@@ -479,28 +482,25 @@
     def product(left, right):
         return jnp.dot(left, right, preferred_element_type=jnp.float32)
 
-    narrow_keys = product(pair_normed[...], g0[...]).astype(jnp.bfloat16)
-    narrow_values = product(pair_normed[...], g1[...]).astype(jnp.bfloat16)
-    hand_over(4)
-    broad_keys = product(pair_normed[...], g2[...]).astype(jnp.bfloat16)
-    broad_values = product(pair_normed[...], g3[...]).astype(jnp.bfloat16)
-    hand_over(5)
-    hand_over(6)
-
-    def attend(query_weights, table, keys, values, plain, out):
+    def project(sums, array, start, width):
+        cols = pl.ds(start, width)
+        sums[:, cols] = product(query_normed, gathered[array][:, cols])
+
+    def rotated(sums, table, start, stop):
+        halfway, cols = ROTARY // 2, pl.ds(start, stop - start)
+        values = sums[:, cols]
+        return (
+            values * table[0, :, cols]
+            + pltpu.roll(values, stop - start - halfway, 1) * table[1, :, cols]
+            + pltpu.roll(values, halfway, 1) * table[2, :, cols]
+        ).astype(jnp.bfloat16)
+
+    def attend(queries, start, keys, values, plain, which):
         width = plain + ROTARY
-        sums = product(query_normed, query_weights[...])
-        total = sums.shape[1]
-        halfway = ROTARY // 2
-        queries = (
-            sums * table[0]
-            + pltpu.roll(sums, total - halfway, 1) * table[1]
-            + pltpu.roll(sums, halfway, 1) * table[2]
-        ).astype(jnp.bfloat16)
         factor = width ** (-0.5) * math.log2(math.e)
         attended = []
-        for head in range(heads):
-            query = queries[:, head * width : (head + 1) * width]
+        for head in which:
+            query = queries[:, head * width - start : (head + 1) * width - start]
             key = jnp.concatenate(
                 [keys[:, head * plain : (head + 1) * plain], rope_keys[...]], axis=1
             )
@@ -513,15 +513,48 @@
                 shifted.astype(jnp.bfloat16), values[:, head * VALUE_SIZE : (head + 1) * VALUE_SIZE]
             )
             attended.append((mixed / totals).astype(jnp.bfloat16).astype(jnp.float32))
+        return attended
+
+    def finish_group(attended, out):
         flat = jnp.concatenate(attended, axis=1)
         scaled = flat * lax.rsqrt(jnp.mean(flat * flat, axis=-1, keepdims=True) + EPSILON)
         out[0] = scaled.astype(jnp.bfloat16)
 
+    project(narrow_sums, NQ, 0, columns_all[NQ])
+    narrow_queries = rotated(narrow_sums, ntab, 0, columns_all[NQ])
+    narrow_keys = product(pair_normed[...], gathered[NK][...]).astype(jnp.bfloat16)
+    narrow_values = product(pair_normed[...], gathered[NV][...]).astype(jnp.bfloat16)
+    relay(6)
+    hand_over(4)
+    complete(3)
+    broad_keys = product(pair_normed[...], gathered[BK][...]).astype(jnp.bfloat16)
+    hand_over(5)
+    finish_group(
+        attend(narrow_queries, 0, narrow_keys, narrow_values, PLAIN_NARROW, range(heads)),
+        narrow_out,
+    )
+    hand_over(6)
     complete(4)
-    attend(g4, ntab, narrow_keys, narrow_values, PLAIN_NARROW, narrow_out)
+    broad_values = product(pair_normed[...], gathered[BV][...]).astype(jnp.bfloat16)
     complete(5)
+    width_broad = PLAIN_BROAD + ROTARY
+    early = split // width_broad
+    project(broad_sums, BQ, 0, split)
+    attended = attend(
+        rotated(broad_sums, btab, 0, split), 0, broad_keys, broad_values, PLAIN_BROAD, range(early)
+    )
     complete(6)
-    attend(g5, btab, broad_keys, broad_values, PLAIN_BROAD, broad_out)
+    project(broad_sums, BQ, split, columns_all[BQ] - split)
+    start = early * width_broad // LANES * LANES
+    attended += attend(
+        rotated(broad_sums, btab, start, columns_all[BQ]),
+        start,
+        broad_keys,
+        broad_values,
+        PLAIN_BROAD,
+        range(early, heads),
+    )
+    finish_group(attended, broad_out)
 
     for index in range(len(pieces)):
         for kind in range(KINDS):
@@ -558,7 +591,7 @@
     pair_rank = keyvalue_latent.shape[2]
     length = tokens * spread
     heads = narrow_value.shape[1] // VALUE_SIZE
-    weights = (narrow_key, narrow_value, broad_key, broad_value, narrow_query, broad_query)
+    weights = (narrow_key, narrow_value, narrow_query, broad_key, broad_value, broad_query)
     peers = lax.axis_size("dp")
     ktab = key_table(length)
     operands = (
@@ -589,6 +622,8 @@
             pltpu.VMEM(ktab.shape, f32),
             pltpu.VMEM((length, pair_rank), bf16),
             pltpu.VMEM((length, ROTARY), bf16),
+            pltpu.VMEM((tokens, narrow_query.shape[1]), f32),
+            pltpu.VMEM((tokens, broad_query.shape[1]), f32),
             pltpu.SemaphoreType.DMA((7, KINDS)),
             pltpu.SemaphoreType.DMA((7, KINDS)),
             pltpu.SemaphoreType.DMA((2, spread, 3)),

time: 30.7 us -> 29.9 us (0.974)
  Pallas kernels: 27.7 us -> 27 us
    pallas_call x1, Pallas kernels: 27.7 us -> 27 us  [fused_call(): pl.pallas_call(functools.partial(fused, spread, heads), out_shape=(out, o...]
where the time goes in v3:
time: 29.9 us; the launch traced here: 29.8 us
  Pallas kernels  27 us (90%)
  local copies, waits for them, and re-layouts  2.14 us (7%)
  between operations  0.65 us (2%)
    pallas_call x1, Pallas kernels, fused_call(): pl.pallas_call(functools.partial(fused, spread, heads), out_shape=(out, o...  27 us
    unnamed x4, local copies, waits for them, and re-layouts  2.14 us

profile of v3, /device:TPU:0, one launch (start us, length us, event | category | flops | bytes accessed | tf_op | source)
XLA Modules:
  0.0 29.8 jit_solution(14004637925059692448)
XLA Ops:
  0.6 27.0 %shard_map.131 = (bf16[1,128,256]{2,1,0:T(8,128)(2,1)}, bf16[1,128,256]{2,1,0:T(8,128)(2,1)}) custom-call(bf16[1,128,768]{2,1,0:T(8,128)(2,1)} %query_hbm.1, bf16[1,128,512]{2,1,0:T(8,128)(2,1)} %pair_hbm.1, bf16[1,32,128]{2,1,0:T(8,128)(2,1)} %bitcast.1, f32[768]{0:T(1024)} %qgain_hbm.1, f32[512]{0:T(512)} %pgain_hbm.1, bf16[64,256]{1,0:T(8,128)(2,1)} %w0.1, ...), custom_call_target="tpu_custom_call" | custom-call | tf_op jit(solution)/shard_map/pallas_call | solution.py:608
  27.6 0.0 copy-start
  27.6 1.5 %copy.16 = bf16[1,128,256]{2,1,0:T(8,128)(2,1)} copy(bf16[1,128,256]{2,1,0:T(8,128)(2,1)} %get-tuple-element.4) | data formatting | bytes 131072
  29.1 0.0 copy-done
  29.1 0.6 %copy.17 = bf16[1,128,256]{2,1,0:T(8,128)(2,1)} copy(bf16[1,128,256]{2,1,0:T(8,128)(2,1)S(1)} %copy-done) | data formatting | bytes 131072
Async XLA Ops:
  27.6 1.5 %copy-start = (bf16[1,128,256]{2,1,0:T(8,128)(2,1)S(1)}, bf16[1,128,256]{2,1,0:T(8,128)(2,1)}, u32[]{:S(2)}) copy-start(bf16[1,128,256]{2,1,0:T(8,128)(2,1)} %get-tuple-element.5) | copy-start | bytes 196612

commit v4 on v3

--- a/solution.py
+++ b/solution.py
@@ -573,6 +573,17 @@
                     along(item, owner, step, False).wait_send()
 
 
+def hand_out(narrow, broad, narrow_out, broad_out, sems):
+    copies = [
+        pltpu.make_async_copy(narrow, narrow_out, sems.at[0]),
+        pltpu.make_async_copy(broad, broad_out, sems.at[1]),
+    ]
+    for copy in copies:
+        copy.start()
+    for copy in copies:
+        copy.wait()
+
+
 def fused_call(
     spread,
     query_latent,
@@ -605,7 +616,7 @@
     )
     out = jax.ShapeDtypeStruct((1, tokens, heads * VALUE_SIZE), jnp.bfloat16)
     bf16, f32 = jnp.bfloat16, jnp.float32
-    return pl.pallas_call(
+    mixed = pl.pallas_call(
         functools.partial(fused, spread, heads),
         out_shape=(out, out),
         in_specs=[pl.BlockSpec(memory_space=pltpu.HBM)] * len(operands),
@@ -632,9 +643,17 @@
             pltpu.SemaphoreType.DMA((6,)),
         ],
         compiler_params=pltpu.CompilerParams(
-            collective_id=0, has_side_effects=True, vmem_limit_bytes=60 * 2**20
+            collective_id=0, has_side_effects=True, vmem_limit_bytes=48 * 2**20
         ),
-    )(*operands)
+    )(*[pltpu.with_memory_space_constraint(operand, pltpu.HBM) for operand in operands])
+    return pl.pallas_call(
+        hand_out,
+        out_shape=(out, out),
+        in_specs=[pl.BlockSpec(memory_space=pltpu.VMEM)] * 2,
+        out_specs=[pl.BlockSpec(memory_space=pltpu.HBM)] * 2,
+        scratch_shapes=[pltpu.SemaphoreType.DMA((2,))],
+        compiler_params=pltpu.CompilerParams(vmem_limit_bytes=2**20),
+    )(*mixed)
 
 
 def solution(mesh):

time: 29.9 us -> 27.8 us (0.930)
  local copies, waits for them, and re-layouts: 2.14 us -> 0 us
    unnamed x4 -> x0, local copies, waits for them, and re-layouts: 2.14 us -> none
    pallas_call x0 -> x1, Pallas kernels: none -> 0.67 us  [fused_call(): pl.pallas_call(hand_out, out_shape=(out, out), in_specs=[pl.BlockSpec(mem...]
    pallas_call x1, Pallas kernels: 27 us -> 26.3 us  [fused_call(): pl.pallas_call(functools.partial(fused, spread, heads), out_shape=(out, o...]
where the time goes in v4:
time: 27.8 us; the launch traced here: 27.7 us
  Pallas kernels  27 us (97%)
  between operations  0.64 us (2%)
    pallas_call x1, Pallas kernels, fused_call(): pl.pallas_call(functools.partial(fused, spread, heads), out_shape=(out, o...  26.3 us
    pallas_call x1, Pallas kernels, fused_call(): pl.pallas_call(hand_out, out_shape=(out, out), in_specs=[pl.BlockSpec(mem...  0.67 us

profile of v4, /device:TPU:0, one launch (start us, length us, event | category | flops | bytes accessed | tf_op | source)
XLA Modules:
  0.0 27.7 jit_solution(2706149556960482356)
XLA Ops:
  0.6 26.3 %shard_map.131 = (bf16[1,128,256]{2,1,0:T(8,128)(2,1)S(1)}, bf16[1,128,256]{2,1,0:T(8,128)(2,1)S(1)}) custom-call(bf16[1,128,768]{2,1,0:T(8,128)(2,1)} %query_hbm.1, bf16[1,128,512]{2,1,0:T(8,128)(2,1)} %pair_hbm.1, bf16[1,32,128]{2,1,0:T(8,128)(2,1)} %bitcast.1, f32[768]{0:T(1024)} %qgain_hbm.1, f32[512]{0:T(512)} %pgain_hbm.1, bf16[64,256]{1,0:T(8,128)(2,1)} %w0.1, ...), custom_call_target="tpu_custom_call" | custom-call | tf_op jit(solution)/shard_map/pallas_call | solution.py:619
  27.0 0.7 %shard_map.132 = (bf16[1,128,256]{2,1,0:T(8,128)(2,1)}, bf16[1,128,256]{2,1,0:T(8,128)(2,1)}) custom-call(bf16[1,128,256]{2,1,0:T(8,128)(2,1)S(1)} %get-tuple-element.4.narrow, bf16[1,128,256]{2,1,0:T(8,128)(2,1)S(1)} %get-tuple-element.5.broad), custom_call_target="tpu_custom_call" | custom-call | tf_op jit(solution)/shard_map/pallas_call | solution.py:649

commit v5 on v4

--- a/solution.py
+++ b/solution.py
@@ -428,7 +428,7 @@
         for kind in (0, 3, 4, 7, 8):
             arrived(index, kind)
 
-    for index in range(4):
+    for index in range(3):
         send_own(index)
 
     def normed(values, gain):
@@ -447,13 +447,14 @@
             table[index] = values
 
     relay(0)
+    send_own(3)
+    relay(1)
     send_own(4)
-    relay(1)
     for item in items:
         relay_along(1, item)
     relay(2)
+    send_own(5)
     relay(3)
-    send_own(5)
     send_own(6)
     hand_over(0)
     hand_over(1)

time: 27.8 us -> 27.2 us (0.978)
  Pallas kernels: 27 us -> 26.4 us
    pallas_call x1, Pallas kernels: 26.3 us -> 25.8 us  [fused_call(): pl.pallas_call(functools.partial(fused, spread, heads), out_shape=(out, o...]
where the time goes in v5:
time: 27.2 us; the launch traced here: 27.1 us
  Pallas kernels  26.4 us (97%)
  between operations  0.64 us (2%)
    pallas_call x1, Pallas kernels, fused_call(): pl.pallas_call(functools.partial(fused, spread, heads), out_shape=(out, o...  25.8 us
    pallas_call x1, Pallas kernels, fused_call(): pl.pallas_call(hand_out, out_shape=(out, out), in_specs=[pl.BlockSpec(mem...  0.67 us

profile of v5, /device:TPU:0, one launch (start us, length us, event | category | flops | bytes accessed | tf_op | source)
XLA Modules:
  0.0 27.1 jit_solution(2637076218793462459)
XLA Ops:
  0.6 25.8 %shard_map.131 = (bf16[1,128,256]{2,1,0:T(8,128)(2,1)S(1)}, bf16[1,128,256]{2,1,0:T(8,128)(2,1)S(1)}) custom-call(bf16[1,128,768]{2,1,0:T(8,128)(2,1)} %query_hbm.1, bf16[1,128,512]{2,1,0:T(8,128)(2,1)} %pair_hbm.1, bf16[1,32,128]{2,1,0:T(8,128)(2,1)} %bitcast.1, f32[768]{0:T(1024)} %qgain_hbm.1, f32[512]{0:T(512)} %pgain_hbm.1, bf16[64,256]{1,0:T(8,128)(2,1)} %w0.1, ...), custom_call_target="tpu_custom_call" | custom-call | tf_op jit(solution)/shard_map/pallas_call | solution.py:620
  26.4 0.7 %shard_map.132 = (bf16[1,128,256]{2,1,0:T(8,128)(2,1)}, bf16[1,128,256]{2,1,0:T(8,128)(2,1)}) custom-call(bf16[1,128,256]{2,1,0:T(8,128)(2,1)S(1)} %get-tuple-element.4.narrow, bf16[1,128,256]{2,1,0:T(8,128)(2,1)S(1)} %get-tuple-element.5.broad), custom_call_target="tpu_custom_call" | custom-call | tf_op jit(solution)/shard_map/pallas_call | solution.py:650
